TPU v7x, 32 devices: a whole 2x2x4 slice. The times are simulated.
32 devices in a mesh: sp: 4 (over z), tp: 8 (over y, x, core).
Axes of the slice: x: 2, y: 2, z: 4, core: 2. Of those that a mesh axis runs over, the one named last changes fastest.
Arguments:
- token_values: bfloat16 [1024, 2048], P('sp', 'tp'), may hold values from -6 to 6
- write_keys: bfloat16 [1024, 1024], P('sp', 'tp'), may hold values from -0.4375 to 0.4375
- read_keys: bfloat16 [1024, 1024], P('sp', 'tp'), may hold values from -0.4375 to 0.4375
- log_decay: float32 [32, 1024], P('tp', 'sp'), may hold values from -0.7 to 0, as said below
- out_gate: bfloat16 [1024, 2048], P('sp', 'tp'), may hold values from -6 to 6
- out_proj: bfloat16 [4096, 2048], P(None, 'tp'), may hold values from -0.125 to 0.125
- mixed: bfloat16 [1024, 4096], P('sp'), may hold values from -6 to 6
- cotangent: bfloat16 [1024, 4096], P('sp'), may hold values from -8 to 8
- route_ids: int32 [1024, 2], P('sp'), may hold values from 0 to 3, all different within a row; in each aligned block of 256 rows (0 to 255, 256 to 511, ...) at most 192 rows name the same one
- route_weights: float32 [1024, 2], P('sp'), may hold values from 0.25 to 1
- w_gate: bfloat16 [4, 4096, 2048], P('sp', None, 'tp'), may hold values from -0.09375 to 0.09375
- w_up: bfloat16 [4, 4096, 2048], P('sp', None, 'tp'), may hold values from -0.09375 to 0.09375
- w_down: bfloat16 [4, 2048, 4096], P('sp', 'tp'), may hold values from -0.125 to 0.125
Outputs:
- value_grad: bfloat16 [1024, 2048], P('sp', 'tp')
- write_grad: bfloat16 [1024, 1024], P('sp', 'tp')
- read_grad: bfloat16 [1024, 1024], P('sp', 'tp')
- gate_grad: bfloat16 [1024, 2048], P('sp', 'tp')
- proj_grad: float32 [4096, 2048], P('sp', 'tp')
- gate_weight_grad: bfloat16 [4, 4096, 2048], P('sp', None, 'tp')
- up_weight_grad: bfloat16 [4, 4096, 2048], P('sp', None, 'tp')
- down_weight_grad: bfloat16 [4, 2048, 4096], P('sp', 'tp')
Inputs may be any that keep to these rules, and one draw needn't show every extreme that they name: `route_ids`: each row names 2 different experts. Within the rows of one device no expert is named more than 192 times, and in every draw some expert is named exactly 192 times by the rows of some device. `log_decay`: every entry is negative.
All inputs are finite; a program needn't handle non-finite values.
Results may differ from a plain program's by a relative error of at most 0.019.
Values may be sent and summed in bfloat16 or wider, within the bound.
A program may use at most 128 MiB of HBM per device.

v0:
```python
import jax
import jax.numpy as jnp
from jax import lax
from jax.sharding import PartitionSpec as P

HEAD_DIM = 64
STATE = 128
F32 = jnp.float32
BF16 = jnp.bfloat16


def dot(a, b, ca=1, cb=0):
    return lax.dot_general(a, b, (((ca,), (cb,)), ((), ())), preferred_element_type=F32)


def shift(x, by):
    n = lax.axis_size("sp")
    return lax.ppermute(x, "sp", [(i, (i + by) % n) for i in range(n)])


def body(
    token_values,
    write_keys,
    read_keys,
    log_decay,
    out_gate,
    out_proj,
    mixed,
    cotangent,
    route_ids,
    route_weights,
    w_gate,
    w_up,
    w_down,
):
    tok, width = mixed.shape
    n = lax.axis_size("sp")
    cap = 3 * tok // n
    share = width // lax.axis_size("tp")
    own = lax.axis_index("sp")
    offset = lax.axis_index("tp") * share
    rel = lax.rem(route_ids - own + n, n)
    hit = rel[:, :, None] == jnp.arange(n, dtype=jnp.int32)[None, None, :]
    member = jnp.any(hit, axis=1)
    weight = jnp.sum(jnp.where(hit, route_weights[:, :, None], 0.0), axis=1)
    order = jnp.arange(tok, dtype=jnp.int32)
    before = (order[:, None] > order[None, :]).astype(BF16)
    slot = dot(before, member.astype(BF16)).astype(jnp.int32)
    slot = jnp.where(member, slot, -1).T
    place = jnp.arange(cap, dtype=jnp.int32)
    chosen = slot[:, None, :] == place[None, :, None]
    onehot = chosen.astype(BF16)
    row_weight = jnp.sum(jnp.where(chosen, weight.T[:, None, :], 0.0), axis=2)
    mixed_part = lax.dynamic_slice_in_dim(mixed, offset, share, 1)
    cot_part = lax.dynamic_slice_in_dim(cotangent, offset, share, 1)
    away = onehot[1:].reshape((n - 1) * cap, tok)
    away_weight = row_weight[1:].reshape((n - 1) * cap, 1)
    send_rows = dot(away, mixed_part).astype(BF16).reshape(n - 1, cap, share)
    send_scaled = (dot(away, cot_part) * away_weight).astype(BF16).reshape(n - 1, cap, share)
    got_rows = jnp.concatenate([shift(send_rows[j - 1], j) for j in range(1, n)], axis=0)
    got_scaled = jnp.concatenate([shift(send_scaled[j - 1], j) for j in range(1, n)], axis=0)
    rem_rows = lax.all_gather(got_rows, "tp", axis=1, tiled=True)
    rem_scaled = lax.all_gather(got_scaled, "tp", axis=1, tiled=True)
    loc_rows = dot(onehot[0], mixed).astype(BF16)
    loc_scaled = (dot(onehot[0], cotangent) * row_weight[0][:, None]).astype(BF16)
    heads = log_decay.shape[0]
    groups = write_keys.shape[1] // STATE
    per_group = heads // groups
    cumul = jnp.cumsum(log_decay, axis=1)
    total = cumul[:, -1]
    tails = jnp.exp(total[:, None] - cumul)
    leads = jnp.exp(cumul)
    values = token_values.astype(F32)
    gate = out_gate.astype(F32)
    sig = jax.nn.sigmoid(gate)
    silu = gate * sig
    causal = order[:, None] >= order[None, :]

    def widen(per_head):
        return jnp.repeat(per_head.T, HEAD_DIM, axis=1)

    tails_wide = widen(tails)
    leads_wide = widen(leads)
    tailed = (values * tails_wide).astype(BF16)

    def cols(a, g):
        k = per_group * HEAD_DIM
        return a[:, g * k : (g + 1) * k]

    def keys(a, g):
        return a[:, g * STATE : (g + 1) * STATE]

    def head(a, h):
        return a[:, h * HEAD_DIM : (h + 1) * HEAD_DIM]

    local_end = jnp.concatenate(
        [dot(cols(tailed, g), keys(write_keys, g), 0, 0) for g in range(groups)], axis=0
    )
    packed = jnp.concatenate(
        [local_end, jnp.broadcast_to(total[:, None], (heads, STATE))], axis=0
    ).astype(BF16)
    lengths = heads * HEAD_DIM
    entering = jnp.zeros((lengths, STATE), F32)
    run = jnp.zeros((heads,), F32)
    for j in range(1, n):
        got = shift(packed, j).astype(F32)
        live = own >= j
        factor = jnp.where(live, jnp.exp(run), 0.0)
        entering = entering + jnp.repeat(factor, HEAD_DIM)[:, None] * got[:lengths]
        run = run + jnp.where(live, got[lengths:, 0], 0.0)
    ahead = [shift(packed[lengths:], -j).astype(F32)[:, 0] for j in range(1, n)]
    entering_b = entering.astype(BF16)
    decay_of, kept, outs = ([], [], [])
    scores = [dot(keys(read_keys, g), keys(write_keys, g), 1, 1) for g in range(groups)]
    for h in range(heads):
        span = cumul[h][:, None] - cumul[h][None, :]
        decay = jnp.exp(jnp.where(causal, span, -jnp.inf))
        decay_of.append(decay)
        kept.append((scores[h // per_group] * decay).astype(BF16))
        outs.append(dot(kept[h], head(token_values, h)))
    carried = jnp.concatenate(
        [
            dot(
                keys(read_keys, g),
                entering_b[g * per_group * HEAD_DIM : (g + 1) * per_group * HEAD_DIM],
                1,
                1,
            )
            for g in range(groups)
        ],
        axis=1,
    )
    y = jnp.concatenate(outs, axis=1) + carried * leads_wide
    gated_b = (y * silu).astype(BF16)

    def both(loc, rem, w, cb):
        return jnp.concatenate([dot(loc, w, 1, cb), dot(rem, w, 1, cb)], axis=0)

    def over_rows(loc, rem, d):
        return (dot(loc, d[:cap], 0, 0) + dot(rem, d[cap:], 0, 0)).astype(BF16)

    gate_pre = both(loc_rows, rem_rows, w_gate[0], 0)
    up_pre = both(loc_rows, rem_rows, w_up[0], 0)
    sigma = jax.nn.sigmoid(gate_pre)
    act_gate = gate_pre * sigma
    hidden = (act_gate * up_pre).astype(BF16)
    d_hidden = both(loc_scaled, rem_scaled, w_down[0], 1)
    d_gate = (d_hidden * up_pre * sigma * (1.0 + gate_pre * (1.0 - sigma))).astype(BF16)
    d_up = (d_hidden * act_gate).astype(BF16)
    portion = (dot(d_gate, w_gate[0], 1, 1) + dot(d_up, w_up[0], 1, 1)).astype(BF16)
    summed = lax.psum_scatter(portion, "tp", scatter_dimension=1, tiled=True)
    grad_gate = over_rows(loc_rows, rem_rows, d_gate)
    grad_up = over_rows(loc_rows, rem_rows, d_up)
    grad_down = (dot(hidden[:cap], loc_scaled, 0, 0) + dot(hidden[cap:], rem_scaled, 0, 0)).astype(
        BF16
    )
    came = [summed[:cap]] + [shift(summed[j * cap : (j + 1) * cap], -j) for j in range(1, n)]
    came = jnp.concatenate(came, axis=0)
    back = dot(onehot.reshape(n * cap, tok), came, 0, 0)
    grad_part = (cot_part.astype(F32) + back).astype(BF16)
    grad_mixed = lax.all_gather(grad_part, "tp", axis=1, tiled=True)
    out_grad = dot(grad_mixed, out_proj)
    proj_part = dot(grad_mixed, gated_b, 0, 0).astype(BF16)
    proj_grad = lax.psum_scatter(proj_part, "sp", scatter_dimension=0, tiled=True).astype(F32)
    outer = out_grad * silu
    outer_b = outer.astype(BF16)
    led = (outer * leads_wide).astype(BF16)
    local_back = jnp.concatenate(
        [dot(cols(led, g), keys(read_keys, g), 0, 0) for g in range(groups)], axis=0
    ).astype(BF16)
    leaving = jnp.zeros((lengths, STATE), F32)
    run = jnp.zeros((heads,), F32)
    for j in range(1, n):
        got = shift(local_back, -j).astype(F32)
        live = own + j < n
        factor = jnp.where(live, jnp.exp(run), 0.0)
        leaving = leaving + jnp.repeat(factor, HEAD_DIM)[:, None] * got
        run = run + jnp.where(live, ahead[j - 1], 0.0)
    leaving_b = leaving.astype(BF16)
    d_values, d_writes, d_reads = ([], [], [])
    for g in range(groups):
        d_scores = 0.0
        for r in range(per_group):
            h = g * per_group + r
            d_scores = d_scores + dot(head(outer_b, h), head(token_values, h), 1, 1) * decay_of[h]
            d_values.append(dot(kept[h], head(outer_b, h), 0, 0))
        d_scores = d_scores.astype(BF16)
        span = slice(g * per_group * HEAD_DIM, (g + 1) * per_group * HEAD_DIM)
        d_reads.append(dot(d_scores, keys(write_keys, g)) + dot(led[:, span], entering_b[span]))
        d_writes.append(
            dot(d_scores, keys(read_keys, g), 0, 0) + dot(tailed[:, span], leaving_b[span])
        )
    from_end = jnp.concatenate(
        [
            dot(
                keys(write_keys, g),
                leaving_b[g * per_group * HEAD_DIM : (g + 1) * per_group * HEAD_DIM],
                1,
                1,
            )
            for g in range(groups)
        ],
        axis=1,
    )
    d_values = jnp.concatenate(d_values, axis=1) + from_end * tails_wide
    d_out_gate = out_grad * y * sig * (1.0 + gate * (1.0 - sig))
    return (
        d_values.astype(BF16),
        jnp.concatenate(d_writes, axis=1).astype(BF16),
        jnp.concatenate(d_reads, axis=1).astype(BF16),
        d_out_gate.astype(BF16),
        proj_grad,
        grad_gate[None],
        grad_up[None],
        grad_down[None],
    )


def solution(mesh):
    return jax.shard_map(
        body,
        mesh=mesh,
        in_specs=(
            P("sp", "tp"),
            P("sp", "tp"),
            P("sp", "tp"),
            P("tp", "sp"),
            P("sp", "tp"),
            P(None, "tp"),
            P("sp", None),
            P("sp", None),
            P("sp", None),
            P("sp", None),
            P("sp", None, "tp"),
            P("sp", None, "tp"),
            P("sp", "tp", None),
        ),
        out_specs=(
            P("sp", "tp"),
            P("sp", "tp"),
            P("sp", "tp"),
            P("sp", "tp"),
            P("sp", "tp"),
            P("sp", None, "tp"),
            P("sp", None, "tp"),
            P("sp", "tp", None),
        ),
        check_vma=False,
    )
```

profile of v0, /device:TPU:0, one launch (start us, length us, event | category | flops | bytes accessed | tf_op | source)
XLA Modules:
  0.0 302.8 jit_solution(12068777380833281221)
XLA Ops:
  9.8 3.1 %collective-permute-start.3 = (bf16[192,512]{1,0:T(8,128)(2,1)S(1)}, bf16[192,512]{1,0:T(8,128)(2,1)S(1)}, u32[]{:S(2)}, u32[]{:S(2)}) collective-permute-start(bf16[192,512]{1,0:T(8,128)(2,1)S(1)} %get-tuple-element.46), channel_id=1, source_target_pairs={{0,8},{8,16},{16,24},{24,0},{1,9},{9,17},{17,25},{25,1},{2,10},{10... | collective-permute-start | bytes 589832 | tf_op jit(solution)/shard_map/ppermute | solution.py:18
  13.0 2.6 collective-permute-start.4
  16.9 4.0 %collective-permute-done.3 = bf16[192,512]{1,0:T(8,128)(2,1)S(1)} collective-permute-done((bf16[192,512]{1,0:T(8,128)(2,1)S(1)}, bf16[192,512]{1,0:T(8,128)(2,1)S(1)}, u32[]{:S(2)}, u32[]{:S(2)}) %collective-permute-start.3) | collective-permute-done | bytes 196640 | tf_op jit(solution)/shard_map/ppermute | solution.py:18
  20.9 7.6 %collective-permute-done.4 = bf16[192,512]{1,0:T(8,128)(2,1)S(1)} collective-permute-done((bf16[192,512]{1,0:T(8,128)(2,1)S(1)}, bf16[192,512]{1,0:T(8,128)(2,1)S(1)}, u32[]{:S(2)}, u32[]{:S(2)}) %collective-permute-start.4) | collective-permute-done | bytes 196640 | tf_op jit(solution)/shard_map/ppermute | solution.py:18
  31.0 4.7 %collective-permute-start = (bf16[192,512]{1,0:T(8,128)(2,1)S(1)}, bf16[192,512]{1,0:T(8,128)(2,1)S(1)}, u32[]{:S(2)}, u32[]{:S(2)}) collective-permute-start(bf16[192,512]{1,0:T(8,128)(2,1)S(1)} %get-tuple-element.43), channel_id=1, source_target_pairs={{0,8},{8,16},{16,24},{24,0},{1,9},{9,17},{17,25},{25,1},{2,10},{10... | collective-permute-start | bytes 589832 | tf_op jit(solution)/shard_map/ppermute | solution.py:18
  38.2 4.5 %collective-permute-done = bf16[192,512]{1,0:T(8,128)(2,1)S(1)} collective-permute-done((bf16[192,512]{1,0:T(8,128)(2,1)S(1)}, bf16[192,512]{1,0:T(8,128)(2,1)S(1)}, u32[]{:S(2)}, u32[]{:S(2)}) %collective-permute-start) | collective-permute-done | bytes 196640 | tf_op jit(solution)/shard_map/ppermute | solution.py:18
  42.7 6.7 %collective-permute-done.1 = bf16[192,512]{1,0:T(8,128)(2,1)S(1)} collective-permute-done((bf16[192,512]{1,0:T(8,128)(2,1)S(1)}, bf16[192,512]{1,0:T(8,128)(2,1)S(1)}, u32[]{:S(2)}, u32[]{:S(2)}) %collective-permute-start.1) | collective-permute-done | bytes 196640 | tf_op jit(solution)/shard_map/ppermute | solution.py:18
  50.3 2.3 convolution_convert_fusion.1
  58.2 14.3 %all-gather.6.cloned.1.call-done = bf16[576,4096]{1,0:T(8,128)(2,1)} async-done(((bf16[576,512]{1,0:T(8,128)(2,1)}), bf16[576,4096]{1,0:T(8,128)(2,1)}) %all-gather.6.cloned.1.call-update) | async-done | bytes 4718608 | tf_op jit(solution)/shard_map/all_gather | solution.py:62
  72.5 5.4 %fusion.14 = f32[576,256]{1,0:T(8,128)} fusion(bf16[576,4096]{1,0:T(8,128)(2,1)} %all-gather.6.cloned.1.call-done, bf16[1,4096,256]{2,1,0:T(8,128)(2,1)} %param.24), kind=kOutput, calls=%fused_computation.21 | convolution fusion | flops 1207959552 | bytes 7405568 | tf_op jit(solution)/shard_map/dot_general | solution.py:13
  77.8 2.2 fusion.9
  80.1 34.0 %all-gather.4.cloned.1.call-done = bf16[576,4096]{1,0:T(8,128)(2,1)} async-done(((bf16[576,512]{1,0:T(8,128)(2,1)}), bf16[576,4096]{1,0:T(8,128)(2,1)}) %all-gather.4.cloned.1.call-update) | async-done | bytes 4718608 | tf_op jit(solution)/shard_map/all_gather | solution.py:63
  114.0 4.5 %fusion.18 = f32[576,256]{1,0:T(8,128)S(1)} fusion(bf16[576,4096]{1,0:T(8,128)(2,1)} %all-gather.4.cloned.1.call-done, bf16[1,256,4096]{2,1,0:T(8,128)(2,1)} %param.25), kind=kOutput, calls=%fused_computation.25 | convolution fusion | flops 1207959552 | bytes 7405568 | tf_op jit(solution)/shard_map/dot_general | solution.py:13
  121.6 5.5 %add_convert_fusion = bf16[768,4096]{1,0:T(8,128)(2,1)} fusion(f32[768,4096]{1,0:T(8,128)S(1)} %fusion.7, bf16[768,256]{1,0:T(8,128)(2,1)} %get-tuple-element.38, bf16[1,4096,256]{2,1,0:T(8,128)(2,1)S(1)} %copy-done.8), kind=kOutput, calls=%fused_computation | convolution fusion | flops 1616904192 | bytes 21364736 | tf_op jit(solution)/shard_map/dot_general | solution.py:13
  132.3 2.4 collective-permute-start.15
  135.2 53.8 %reduce-scatter.3.cloned.1.call-done = bf16[768,512]{1,0:T(8,128)(2,1)} async-done(((bf16[768,4096]{1,0:T(8,128)(2,1)}), bf16[768,512]{1,0:T(8,128)(2,1)}) %reduce-scatter.3.cloned.1.call-update) | async-done | bytes 786448 | tf_op jit(solution)/shard_map/reduce_scatter | solution.py:151
  190.2 3.4 %collective-permute-start.6 = (bf16[192,512]{1,0:T(8,128)(2,1)S(1)}, bf16[192,512]{1,0:T(8,128)(2,1)S(1)}, u32[]{:S(2)}, u32[]{:S(2)}) collective-permute-start(bf16[192,512]{1,0:T(8,128)(2,1)S(1)} %get-tuple-element.42), channel_id=1, source_target_pairs={{0,24},{8,0},{16,8},{24,16},{1,25},{9,1},{17,9},{25,17},{2,26},{10... | collective-permute-start | bytes 589832 | tf_op jit(solution)/shard_map/ppermute | solution.py:18
  194.8 4.2 %collective-permute-done.6 = bf16[192,512]{1,0:T(8,128)(2,1)S(1)} collective-permute-done((bf16[192,512]{1,0:T(8,128)(2,1)S(1)}, bf16[192,512]{1,0:T(8,128)(2,1)S(1)}, u32[]{:S(2)}, u32[]{:S(2)}) %collective-permute-start.6) | collective-permute-done | bytes 196640 | tf_op jit(solution)/shard_map/ppermute | solution.py:18
  199.0 4.3 %collective-permute-start.16 = (bf16[260,128]{1,0:T(8,128)(2,1)}, bf16[260,128]{1,0:T(8,128)(2,1)}, u32[]{:S(2)}, u32[]{:S(2)}) collective-permute-start(bf16[260,128]{1,0:T(8,128)(2,1)} %pad_maximum_fusion.5), channel_id=1, source_target_pairs={{0,24},{8,0},{16,8},{24,16},{1,25},{9,1},{17,9},{25,17},{2,26},{10... | collective-permute-start | bytes 199688 | tf_op jit(solution)/shard_map/ppermute | solution.py:18
  203.3 7.8 %collective-permute-done.7 = bf16[192,512]{1,0:T(8,128)(2,1)S(1)} collective-permute-done((bf16[192,512]{1,0:T(8,128)(2,1)S(1)}, bf16[192,512]{1,0:T(8,128)(2,1)S(1)}, u32[]{:S(2)}, u32[]{:S(2)}) %collective-permute-start.7) | collective-permute-done | bytes 196640 | tf_op jit(solution)/shard_map/ppermute | solution.py:18
  211.2 3.3 %collective-permute-start.12 = (bf16[4,128]{1,0:T(4,128)(2,1)S(1)}, bf16[4,128]{1,0:T(4,128)(2,1)}, u32[]{:S(2)}, u32[]{:S(2)}) collective-permute-start(bf16[4,128]{1,0:T(4,128)(2,1)S(1)} %broadcast_in_dim.99), channel_id=1, source_target_pairs={{0,16},{8,24},{16,0},{24,8},{1,17},{9,25},{17,1},{25,9},{2,18},{10... | collective-permute-start | bytes 3080 | tf_op jit(solution)/shard_map/ppermute | solution.py:18
  214.5 2.1 fusion.23
  230.7 3.2 %fusion.4 = bf16[1,256,4096]{2,1,0:T(8,128)(2,1)} fusion(f32[256,4096]{1,0:T(8,128)S(1)} %fusion.60, bf16[576,4096]{1,0:T(8,128)(2,1)S(1)} %bitcast.122, bf16[768,256]{1,0:T(8,128)(2,1)S(1)} %get-tuple-element.36), kind=kOutput, calls=%fused_computation.11 | convolution fusion | flops 1210056704 | bytes 11304960 | tf_op jit(solution)/shard_map/dot_general | solution.py:13
  233.9 3.2 %fusion.5 = bf16[1,4096,256]{2,1,0:T(8,128)(2,1)} fusion(f32[4096,256]{1,0:T(8,128)S(1)} %fusion.62, bf16[576,4096]{1,0:T(8,128)(2,1)S(1)} %bitcast.133, bf16[768,256]{1,0:T(8,128)(2,1)S(1)} %copy-done.12), kind=kOutput, calls=%fused_computation.12 | convolution fusion | flops 1210056704 | bytes 11304960 | tf_op jit(solution)/shard_map/dot_general | solution.py:13
  237.1 5.4 %all-gather.8.cloned.1.call-done = bf16[256,4096]{1,0:T(8,128)(2,1)} async-done(((bf16[256,512]{1,0:T(8,128)(2,1)}), bf16[256,4096]{1,0:T(8,128)(2,1)}) %all-gather.8.cloned.1.call-update) | async-done | bytes 2097168 | tf_op jit(solution)/shard_map/all_gather | solution.py:161
  242.5 3.7 %convolution_convert_fusion = bf16[4096,256]{1,0:T(8,128)(2,1)} fusion(bf16[256,4096]{1,0:T(8,128)(2,1)} %all-gather.8.cloned.1.call-done, f32[256,256]{0,1:T(8,128)S(1)} %fusion.25, bf16[256,256]{0,1:T(8,128)(2,1)S(1)} %copy.41), kind=kOutput, calls=%fused_computation.8 | convolution fusion | flops 538378240 | bytes 4587520 | tf_op jit(solution)/shard_map/dot_general | solution.py:13
  247.0 5.7 %fusion.6 = bf16[1,4096,256]{2,1,0:T(8,128)(2,1)} fusion(f32[4096,256]{1,0:T(8,128)S(1)} %fusion.64, bf16[576,4096]{1,0:T(8,128)(2,1)} %all-gather.6.cloned.1.call-done, bf16[768,256]{1,0:T(8,128)(2,1)S(1)} %get-tuple-element.37), kind=kOutput, calls=%fused_computation.13 | convolution fusion | flops 1210056704 | bytes 11304960 | tf_op jit(solution)/shard_map/dot_general | solution.py:13
  253.9 2.5 collective-permute-start.11
  257.9 2.3 collective-permute-start.9
  264.3 2.0 collective-permute-done.11
  270.1 24.1 %reduce-scatter.5.cloned.1.call-done = bf16[1024,256]{1,0:T(8,128)(2,1)} async-done(((bf16[4096,256]{1,0:T(8,128)(2,1)}), bf16[1024,256]{1,0:T(8,128)(2,1)}) %reduce-scatter.5.cloned.1.call-update) | async-done | bytes 524304 | tf_op jit(solution)/shard_map/reduce_scatter | solution.py:164
  294.2 2.1 convert_element_type.159
  (198 shorter events, 51.6 us)
Async XLA Ops:
  7.2 46.1 %copy-start = (bf16[1,4096,256]{2,1,0:T(8,128)(2,1)S(1)}, bf16[1,4096,256]{2,1,0:T(8,128)(2,1)}, u32[]{:S(2)}) copy-start(bf16[1,4096,256]{2,1,0:T(8,128)(2,1)} %param.23) | copy-start | bytes 6291460
  7.2 65.3 %all-gather.6.cloned.1.call-start = ((), (), s32[]{:S(2)}) async-start(), calls=%async_computation.3 | async-start | bytes 5308416 | tf_op jit(solution)/shard_map/all_gather | solution.py:62
  8.4 21.0 %copy-start.30 = (f32[256,2]{0,1:T(2,128)S(1)}, f32[256,2]{0,1:T(2,128)}, u32[]{:S(2)}) copy-start(f32[256,2]{0,1:T(2,128)} %param.22) | copy-start | bytes 6148
  9.8 11.0 %collective-permute-start.3 = (bf16[192,512]{1,0:T(8,128)(2,1)S(1)}, bf16[192,512]{1,0:T(8,128)(2,1)S(1)}, u32[]{:S(2)}, u32[]{:S(2)}) collective-permute-start(bf16[192,512]{1,0:T(8,128)(2,1)S(1)} %get-tuple-element.46), channel_id=1, source_target_pairs={{0,8},{8,16},{16,24},{24,0},{1,9},{9,17},{17,25},{25,1},{2,10},{10... | collective-permute-start | bytes 589832 | tf_op jit(solution)/shard_map/ppermute | solution.py:18
  13.0 15.5 %collective-permute-start.4 = (bf16[192,512]{1,0:T(8,128)(2,1)S(1)}, bf16[192,512]{1,0:T(8,128)(2,1)S(1)}, u32[]{:S(2)}, u32[]{:S(2)}) collective-permute-start(bf16[192,512]{1,0:T(8,128)(2,1)S(1)} %get-tuple-element.48), channel_id=1, source_target_pairs={{0,16},{8,24},{16,0},{24,8},{1,17},{9,25},{17,1},{25,9},{2,18},{10... | collective-permute-start | bytes 589832 | tf_op jit(solution)/shard_map/ppermute | solution.py:18
  15.5 12.9 %collective-permute-start.5 = (bf16[192,512]{1,0:T(8,128)(2,1)S(1)}, bf16[192,512]{1,0:T(8,128)(2,1)S(1)}, u32[]{:S(2)}, u32[]{:S(2)}) collective-permute-start(bf16[192,512]{1,0:T(8,128)(2,1)S(1)} %get-tuple-element.47), channel_id=1, source_target_pairs={{0,24},{8,0},{16,8},{24,16},{1,25},{9,1},{17,9},{25,17},{2,26},{10... | collective-permute-start | bytes 589832 | tf_op jit(solution)/shard_map/ppermute | solution.py:18
  29.3 84.7 %all-gather.4.cloned.1.call-start = ((), (), s32[]{:S(2)}) async-start(), calls=%async_computation.2 | async-start | bytes 5308416 | tf_op jit(solution)/shard_map/all_gather | solution.py:63
  31.0 11.6 %collective-permute-start = (bf16[192,512]{1,0:T(8,128)(2,1)S(1)}, bf16[192,512]{1,0:T(8,128)(2,1)S(1)}, u32[]{:S(2)}, u32[]{:S(2)}) collective-permute-start(bf16[192,512]{1,0:T(8,128)(2,1)S(1)} %get-tuple-element.43), channel_id=1, source_target_pairs={{0,8},{8,16},{16,24},{24,0},{1,9},{9,17},{17,25},{25,1},{2,10},{10... | collective-permute-start | bytes 589832 | tf_op jit(solution)/shard_map/ppermute | solution.py:18
  35.8 13.6 %collective-permute-start.1 = (bf16[192,512]{1,0:T(8,128)(2,1)S(1)}, bf16[192,512]{1,0:T(8,128)(2,1)S(1)}, u32[]{:S(2)}, u32[]{:S(2)}) collective-permute-start(bf16[192,512]{1,0:T(8,128)(2,1)S(1)} %get-tuple-element.45), channel_id=1, source_target_pairs={{0,16},{8,24},{16,0},{24,8},{1,17},{9,25},{17,1},{25,9},{2,18},{10... | collective-permute-start | bytes 589832 | tf_op jit(solution)/shard_map/ppermute | solution.py:18
  37.4 12.0 %collective-permute-start.2 = (bf16[192,512]{1,0:T(8,128)(2,1)S(1)}, bf16[192,512]{1,0:T(8,128)(2,1)S(1)}, u32[]{:S(2)}, u32[]{:S(2)}) collective-permute-start(bf16[192,512]{1,0:T(8,128)(2,1)S(1)} %get-tuple-element.44), channel_id=1, source_target_pairs={{0,24},{8,0},{16,8},{24,16},{1,25},{9,1},{17,9},{25,17},{2,26},{10... | collective-permute-start | bytes 589832 | tf_op jit(solution)/shard_map/ppermute | solution.py:18
  50.3 138.7 %reduce-scatter.3.cloned.1.call-start = ((), (), s32[]{:S(2)}) async-start(), calls=%async_computation.4 | async-start | bytes 7077888 | tf_op jit(solution)/shard_map/reduce_scatter | solution.py:151
  127.2 7.8 %copy-start.13 = (bf16[256,128]{1,0:T(8,128)(2,1)S(1)}, bf16[256,128]{1,0:T(8,128)(2,1)}, u32[]{:S(2)}) copy-start(bf16[256,128]{1,0:T(8,128)(2,1)} %param.15) | copy-start | bytes 196612
  127.2 115.3 %all-gather.8.cloned.1.call-start = ((), (), s32[]{:S(2)}) async-start(), calls=%async_computation.5 | async-start | bytes 2359296 | tf_op jit(solution)/shard_map/all_gather | solution.py:161
  130.8 92.3 %collective-permute-start.14 = (bf16[260,128]{1,0:T(8,128)(2,1)}, bf16[260,128]{1,0:T(8,128)(2,1)}, u32[]{:S(2)}, u32[]{:S(2)}) collective-permute-start(bf16[260,128]{1,0:T(8,128)(2,1)} %pad_maximum_fusion.5), channel_id=1, source_target_pairs={{0,8},{8,16},{16,24},{24,0},{1,9},{9,17},{17,25},{25,1},{2,10},{10... | collective-permute-start | bytes 199688 | tf_op jit(solution)/shard_map/ppermute | solution.py:18
  132.3 91.7 %collective-permute-start.15 = (bf16[260,128]{1,0:T(8,128)(2,1)}, bf16[260,128]{1,0:T(8,128)(2,1)}, u32[]{:S(2)}, u32[]{:S(2)}) collective-permute-start(bf16[260,128]{1,0:T(8,128)(2,1)} %pad_maximum_fusion.5), channel_id=1, source_target_pairs={{0,16},{8,24},{16,0},{24,8},{1,17},{9,25},{17,1},{25,9},{2,18},{10... | collective-permute-start | bytes 199688 | tf_op jit(solution)/shard_map/ppermute | solution.py:18
  135.2 84.3 %copy-start.22 = (f32[256,256]{1,0:T(8,128)}, f32[256,256]{1,0:T(8,128)S(1)}, u32[]{:S(2)}) copy-start(f32[256,256]{1,0:T(8,128)S(1)} %fusion.102) | copy-start | bytes 786436
  190.2 8.7 %collective-permute-start.6 = (bf16[192,512]{1,0:T(8,128)(2,1)S(1)}, bf16[192,512]{1,0:T(8,128)(2,1)S(1)}, u32[]{:S(2)}, u32[]{:S(2)}) collective-permute-start(bf16[192,512]{1,0:T(8,128)(2,1)S(1)} %get-tuple-element.42), channel_id=1, source_target_pairs={{0,24},{8,0},{16,8},{24,16},{1,25},{9,1},{17,9},{25,17},{2,26},{10... | collective-permute-start | bytes 589832 | tf_op jit(solution)/shard_map/ppermute | solution.py:18
  193.6 17.4 %collective-permute-start.7 = (bf16[192,512]{1,0:T(8,128)(2,1)S(1)}, bf16[192,512]{1,0:T(8,128)(2,1)S(1)}, u32[]{:S(2)}, u32[]{:S(2)}) collective-permute-start(bf16[192,512]{1,0:T(8,128)(2,1)S(1)} %get-tuple-element.41), channel_id=1, source_target_pairs={{0,16},{8,24},{16,0},{24,8},{1,17},{9,25},{17,1},{25,9},{2,18},{10... | collective-permute-start | bytes 589832 | tf_op jit(solution)/shard_map/ppermute | solution.py:18
  193.6 17.6 %collective-permute-start.8 = (bf16[192,512]{1,0:T(8,128)(2,1)S(1)}, bf16[192,512]{1,0:T(8,128)(2,1)S(1)}, u32[]{:S(2)}, u32[]{:S(2)}) collective-permute-start(bf16[192,512]{1,0:T(8,128)(2,1)S(1)} %get-tuple-element.40), channel_id=1, source_target_pairs={{0,8},{8,16},{16,24},{24,0},{1,9},{9,17},{17,25},{25,1},{2,10},{10... | collective-permute-start | bytes 589832 | tf_op jit(solution)/shard_map/ppermute | solution.py:18
  199.0 27.1 %collective-permute-start.16 = (bf16[260,128]{1,0:T(8,128)(2,1)}, bf16[260,128]{1,0:T(8,128)(2,1)}, u32[]{:S(2)}, u32[]{:S(2)}) collective-permute-start(bf16[260,128]{1,0:T(8,128)(2,1)} %pad_maximum_fusion.5), channel_id=1, source_target_pairs={{0,24},{8,0},{16,8},{24,16},{1,25},{9,1},{17,9},{25,17},{2,26},{10... | collective-permute-start | bytes 199688 | tf_op jit(solution)/shard_map/ppermute | solution.py:18
  211.1 10.3 %collective-permute-start.10 = (bf16[4,128]{1,0:T(4,128)(2,1)S(1)}, bf16[4,128]{1,0:T(4,128)(2,1)}, u32[]{:S(2)}, u32[]{:S(2)}) collective-permute-start(bf16[4,128]{1,0:T(4,128)(2,1)S(1)} %broadcast_in_dim.99), channel_id=1, source_target_pairs={{0,24},{8,0},{16,8},{24,16},{1,25},{9,1},{17,9},{25,17},{2,26},{10... | collective-permute-start | bytes 3080 | tf_op jit(solution)/shard_map/ppermute | solution.py:18
  211.2 10.2 %collective-permute-start.12 = (bf16[4,128]{1,0:T(4,128)(2,1)S(1)}, bf16[4,128]{1,0:T(4,128)(2,1)}, u32[]{:S(2)}, u32[]{:S(2)}) collective-permute-start(bf16[4,128]{1,0:T(4,128)(2,1)S(1)} %broadcast_in_dim.99), channel_id=1, source_target_pairs={{0,16},{8,24},{16,0},{24,8},{1,17},{9,25},{17,1},{25,9},{2,18},{10... | collective-permute-start | bytes 3080 | tf_op jit(solution)/shard_map/ppermute | solution.py:18
  216.6 11.8 %copy-start.3 = (bf16[192,4096]{1,0:T(8,128)(2,1)S(1)}, bf16[192,4096]{1,0:T(8,128)(2,1)}, u32[]{:S(2)}) copy-start(bf16[192,4096]{1,0:T(8,128)(2,1)} %copy-done.2) | copy-start | bytes 4718596
  216.6 11.8 %copy-start.12 = (bf16[768,256]{1,0:T(8,128)(2,1)S(1)}, bf16[768,256]{1,0:T(8,128)(2,1)}, u32[]{:S(2)}) copy-start(bf16[768,256]{1,0:T(8,128)(2,1)} %get-tuple-element.38) | copy-start | bytes 1179652
  216.6 77.6 %reduce-scatter.5.cloned.1.call-start = ((), (), s32[]{:S(2)}) async-start(), calls=%async_computation.6 | async-start | bytes 2621440 | tf_op jit(solution)/shard_map/reduce_scatter | solution.py:164
  252.7 7.7 %copy-start.28 = (f32[256]{0:T(256)S(1)}, f32[256]{0:T(256)}, u32[]{:S(2)}) copy-start(f32[256]{0:T(256)} %copy-done.27) | copy-start | bytes 3076
  252.7 8.0 %copy-start.26 = (f32[256]{0:T(256)S(1)}, f32[256]{0:T(256)}, u32[]{:S(2)}) copy-start(f32[256]{0:T(256)} %copy-done.25) | copy-start | bytes 3076
  252.8 8.2 %copy-start.32 = (f32[256]{0:T(256)S(1)}, f32[256]{0:T(256)}, u32[]{:S(2)}) copy-start(f32[256]{0:T(256)} %copy-done.31) | copy-start | bytes 3076
  253.9 12.3 %collective-permute-start.11 = (bf16[256,128]{1,0:T(8,128)(2,1)S(1)}, bf16[256,128]{1,0:T(8,128)(2,1)S(1)}, u32[]{:S(2)}, u32[]{:S(2)}) collective-permute-start(bf16[256,128]{1,0:T(8,128)(2,1)S(1)} %convolution_convert_fusion.4), channel_id=1, source_target_pairs={{0,16},{8,24},{16,0},{24,8},{1,17},{9,25},{17,1},{25,9},{2,18},{10... | collective-permute-start | bytes 196616 | tf_op jit(solution)/shard_map/ppermute | solution.py:18
  256.4 9.8 %collective-permute-start.13 = (bf16[256,128]{1,0:T(8,128)(2,1)S(1)}, bf16[256,128]{1,0:T(8,128)(2,1)S(1)}, u32[]{:S(2)}, u32[]{:S(2)}) collective-permute-start(bf16[256,128]{1,0:T(8,128)(2,1)S(1)} %convolution_convert_fusion.4), channel_id=1, source_target_pairs={{0,8},{8,16},{16,24},{24,0},{1,9},{9,17},{17,25},{25,1},{2,10},{10... | collective-permute-start | bytes 196616 | tf_op jit(solution)/shard_map/ppermute | solution.py:18
  257.9 10.2 %collective-permute-start.9 = (bf16[256,128]{1,0:T(8,128)(2,1)S(1)}, bf16[256,128]{1,0:T(8,128)(2,1)S(1)}, u32[]{:S(2)}, u32[]{:S(2)}) collective-permute-start(bf16[256,128]{1,0:T(8,128)(2,1)S(1)} %convolution_convert_fusion.4), channel_id=1, source_target_pairs={{0,24},{8,0},{16,8},{24,16},{1,25},{9,1},{17,9},{25,17},{2,26},{10... | collective-permute-start | bytes 196616 | tf_op jit(solution)/shard_map/ppermute | solution.py:18
  262.4 33.9 %copy-start.1 = (bf16[1,4096,256]{2,1,0:T(8,128)(2,1)S(1)}, bf16[1,4096,256]{2,1,0:T(8,128)(2,1)}, u32[]{:S(2)}) copy-start(bf16[1,4096,256]{2,1,0:T(8,128)(2,1)} %param.23) | copy-start | bytes 6291460
  (30 other events, 108.0 us)
Sparse Core Ops, SparseCore 0:
  29.4 43.0 all-gather.5
  74.4 39.6 all-gather.3
  127.3 61.5 reduce-scatter.2
  216.7 25.7 all-gather.7
  246.3 47.8 reduce-scatter.4
where the time goes:
time: 303 us
  waiting for transfers between devices  170 us (56%)
  matrix products  58 us (19%)
  starting transfers between devices  36.9 us (12%)
  between operations  14.5 us (5%)
  other arithmetic  12.4 us (4%)
  local copies, waits for them, and re-layouts  10.9 us (4%)
    dot_general x43, matrix products, dot(): lax.dot_general(a, b, (((ca,), (cb,)), ((), ())), preferred_element_type=...  58 us
    reduce_scatter x1, waiting for transfers between devices, body(): summed = lax.psum_scatter(portion, 'tp', scatter_dimension=1, tiled=True)  53.8 us
    ppermute x17, waiting for transfers between devices, shift(): return lax.ppermute(x, 'sp', [(i, (i + by) % n) for i in range(n)])  38.5 us
    ppermute x17, starting transfers between devices, shift(): return lax.ppermute(x, 'sp', [(i, (i + by) % n) for i in range(n)])  36.7 us
    all_gather x1, waiting for transfers between devices, body(): rem_scaled = lax.all_gather(got_scaled, 'tp', axis=1, tiled=True)  34 us
    reduce_scatter x1, waiting for transfers between devices, body(): lax.psum_scatter(proj_part, 'sp', scatter_dimension=0, tiled=True)  24.1 us
    all_gather x1, waiting for transfers between devices, body(): rem_rows = lax.all_gather(got_rows, 'tp', axis=1, tiled=True)  14.3 us
    unnamed x86, local copies, waits for them, and re-layouts  7.65 us
  transfers between devices with their start and end apart: 22, of which 13 were waited for; matrix products, arithmetic and copies ran while one was open for 18% of the time, Pallas kernels for 0%

commit v1 on v0

--- a/solution.py
+++ b/solution.py
@@ -60,7 +60,12 @@
     got_rows = jnp.concatenate([shift(send_rows[j - 1], j) for j in range(1, n)], axis=0)
     got_scaled = jnp.concatenate([shift(send_scaled[j - 1], j) for j in range(1, n)], axis=0)
     rem_rows = lax.all_gather(got_rows, "tp", axis=1, tiled=True)
-    rem_scaled = lax.all_gather(got_scaled, "tp", axis=1, tiled=True)
+    ring = [got_scaled]
+    for hop in range(7):
+        ring.append(lax.ppermute(ring[-1], "tp", [(dev, (dev + 1) % 8) for dev in range(8)]))
+    rem_scaled = jnp.roll(
+        jnp.concatenate(ring[::-1], axis=1), (lax.axis_index("tp") + 1) * ring[0].shape[1], axis=1
+    )
     loc_rows = dot(onehot[0], mixed).astype(BF16)
     loc_scaled = (dot(onehot[0], cotangent) * row_weight[0][:, None]).astype(BF16)
     heads = log_decay.shape[0]

time: 303 us -> 340 us (1.12)
  waiting for transfers between devices: 170 us -> 197 us
  local copies, waits for them, and re-layouts: 10.9 us -> 18.6 us
    ppermute x0 -> x7, waiting for transfers between devices: none -> 72.3 us  [body(): lax.ppermute(ring[-1], 'tp', [(dev, (dev + 1) % 8) for dev in range(8)])]
    all_gather x1 -> x0, waiting for transfers between devices: 34 us -> none  [body(): rem_scaled = lax.all_gather(got_scaled, 'tp', axis=1, tiled=True)]
    all_gather x1, waiting for transfers between devices: 14.3 us -> 0.01 us  [body(): rem_rows = lax.all_gather(got_rows, 'tp', axis=1, tiled=True)]
    unnamed x86 -> x147, local copies, waits for them, and re-layouts: 7.65 us -> 15.8 us
    ppermute x17, waiting for transfers between devices: 38.5 us -> 43.1 us  [shift(): return lax.ppermute(x, 'sp', [(i, (i + by) % n) for i in range(n)])]
  transfers between devices with their start and end apart: 22 -> 28, of which waited for: 13 -> 17; matrix products, arithmetic and copies ran while one was open for 18% -> 17% of each run, Pallas kernels for 0% -> 0%
where the time goes in v1:
time: 340 us; the launch traced here: 339 us
  waiting for transfers between devices  197 us (58%)
  matrix products  57.7 us (17%)
  starting transfers between devices  39.7 us (12%)
  local copies, waits for them, and re-layouts  18.6 us (5%)
  between operations  14.9 us (4%)
  other arithmetic  11.6 us (3%)
    ppermute x7, waiting for transfers between devices, body(): lax.ppermute(ring[-1], 'tp', [(dev, (dev + 1) % 8) for dev in range(8)])  72.3 us
    dot_general x43, matrix products, dot(): lax.dot_general(a, b, (((ca,), (cb,)), ((), ())), preferred_element_type=...  57.7 us
    reduce_scatter x1, waiting for transfers between devices, body(): summed = lax.psum_scatter(portion, 'tp', scatter_dimension=1, tiled=True)  55 us
    ppermute x17, waiting for transfers between devices, shift(): return lax.ppermute(x, 'sp', [(i, (i + by) % n) for i in range(n)])  43.1 us
    ppermute x17, starting transfers between devices, shift(): return lax.ppermute(x, 'sp', [(i, (i + by) % n) for i in range(n)])  38.6 us
    reduce_scatter x1, waiting for transfers between devices, body(): lax.psum_scatter(proj_part, 'sp', scatter_dimension=0, tiled=True)  21.2 us
    unnamed x147, local copies, waits for them, and re-layouts  15.8 us
  transfers between devices with their start and end apart: 28, of which 17 were waited for; matrix products, arithmetic and copies ran while one was open for 17% of the time, Pallas kernels for 0%

profile of v1, /device:TPU:0, one launch (start us, length us, event | category | flops | bytes accessed | tf_op | source)
XLA Modules:
  0.0 339.5 jit_solution(16410928422816186037)
XLA Ops:
  10.5 3.1 collective-permute-start.10
  13.6 2.6 collective-permute-start.11
  17.6 4.0 %collective-permute-done.10 = bf16[192,512]{1,0:T(8,128)(2,1)S(1)} collective-permute-done((bf16[192,512]{1,0:T(8,128)(2,1)S(1)}, bf16[192,512]{1,0:T(8,128)(2,1)S(1)}, u32[]{:S(2)}, u32[]{:S(2)}) %collective-permute-start.10) | collective-permute-done | bytes 196640 | tf_op jit(solution)/shard_map/ppermute | solution.py:18
  21.5 7.6 %collective-permute-done.11 = bf16[192,512]{1,0:T(8,128)(2,1)S(1)} collective-permute-done((bf16[192,512]{1,0:T(8,128)(2,1)S(1)}, bf16[192,512]{1,0:T(8,128)(2,1)S(1)}, u32[]{:S(2)}, u32[]{:S(2)}) %collective-permute-start.11) | collective-permute-done | bytes 196640 | tf_op jit(solution)/shard_map/ppermute | solution.py:18
  31.7 4.7 %collective-permute-start = (bf16[192,512]{1,0:T(8,128)(2,1)S(1)}, bf16[192,512]{1,0:T(8,128)(2,1)S(1)}, u32[]{:S(2)}, u32[]{:S(2)}) collective-permute-start(bf16[192,512]{1,0:T(8,128)(2,1)S(1)} %get-tuple-element.43), channel_id=1, source_target_pairs={{0,8},{8,16},{16,24},{24,0},{1,9},{9,17},{17,25},{25,1},{2,10},{10... | collective-permute-start | bytes 589832 | tf_op jit(solution)/shard_map/ppermute | solution.py:18
  38.9 4.5 %collective-permute-done = bf16[192,512]{1,0:T(8,128)(2,1)S(1)} collective-permute-done((bf16[192,512]{1,0:T(8,128)(2,1)S(1)}, bf16[192,512]{1,0:T(8,128)(2,1)S(1)}, u32[]{:S(2)}, u32[]{:S(2)}) %collective-permute-start) | collective-permute-done | bytes 196640 | tf_op jit(solution)/shard_map/ppermute | solution.py:18
  43.3 6.7 %collective-permute-done.1 = bf16[192,512]{1,0:T(8,128)(2,1)S(1)} collective-permute-done((bf16[192,512]{1,0:T(8,128)(2,1)S(1)}, bf16[192,512]{1,0:T(8,128)(2,1)S(1)}, u32[]{:S(2)}, u32[]{:S(2)}) %collective-permute-start.1) | collective-permute-done | bytes 196640 | tf_op jit(solution)/shard_map/ppermute | solution.py:18
  50.2 13.3 %collective-permute-done.3 = bf16[576,512]{1,0:T(8,128)(2,1)S(1)} collective-permute-done((bf16[576,512]{1,0:T(8,128)(2,1)S(1)}, bf16[576,512]{1,0:T(8,128)(2,1)S(1)}, u32[]{:S(2)}, u32[]{:S(2)}) %collective-permute-start.3) | collective-permute-done | bytes 589856 | tf_op jit(solution)/shard_map/ppermute | solution.py:65
  64.1 15.3 %collective-permute-done.4 = bf16[576,512]{1,0:T(8,128)(2,1)S(1)} collective-permute-done((bf16[576,512]{1,0:T(8,128)(2,1)S(1)}, bf16[576,512]{1,0:T(8,128)(2,1)S(1)}, u32[]{:S(2)}, u32[]{:S(2)}) %collective-permute-start.4) | collective-permute-done | bytes 589856 | tf_op jit(solution)/shard_map/ppermute | solution.py:65
  79.3 10.2 %collective-permute-done.5 = bf16[576,512]{1,0:T(8,128)(2,1)S(1)} collective-permute-done((bf16[576,512]{1,0:T(8,128)(2,1)S(1)}, bf16[576,512]{1,0:T(8,128)(2,1)S(1)}, u32[]{:S(2)}, u32[]{:S(2)}) %collective-permute-start.5) | collective-permute-done | bytes 589856 | tf_op jit(solution)/shard_map/ppermute | solution.py:65
  90.3 10.3 %collective-permute-done.6 = bf16[576,512]{1,0:T(8,128)(2,1)} collective-permute-done((bf16[576,512]{1,0:T(8,128)(2,1)S(1)}, bf16[576,512]{1,0:T(8,128)(2,1)}, u32[]{:S(2)}, u32[]{:S(2)}) %collective-permute-start.6) | collective-permute-done | bytes 589856 | tf_op jit(solution)/shard_map/ppermute | solution.py:65
  103.0 8.2 %collective-permute-done.7 = bf16[576,512]{1,0:T(8,128)(2,1)} collective-permute-done((bf16[576,512]{1,0:T(8,128)(2,1)}, bf16[576,512]{1,0:T(8,128)(2,1)}, u32[]{:S(2)}, u32[]{:S(2)}) %collective-permute-start.7) | collective-permute-done | bytes 589856 | tf_op jit(solution)/shard_map/ppermute | solution.py:65
  113.8 7.8 %collective-permute-done.8 = bf16[576,512]{1,0:T(8,128)(2,1)S(1)} collective-permute-done((bf16[576,512]{1,0:T(8,128)(2,1)}, bf16[576,512]{1,0:T(8,128)(2,1)S(1)}, u32[]{:S(2)}, u32[]{:S(2)}) %collective-permute-start.8) | collective-permute-done | bytes 589856 | tf_op jit(solution)/shard_map/ppermute | solution.py:65
  124.5 7.3 %collective-permute-done.9 = bf16[576,512]{1,0:T(8,128)(2,1)S(1)} collective-permute-done((bf16[576,512]{1,0:T(8,128)(2,1)S(1)}, bf16[576,512]{1,0:T(8,128)(2,1)S(1)}, u32[]{:S(2)}, u32[]{:S(2)}) %collective-permute-start.9) | collective-permute-done | bytes 589856 | tf_op jit(solution)/shard_map/ppermute | solution.py:65
  137.5 3.7 %copy-done.9 = bf16[576,8192]{1,0:T(8,128)(2,1)} copy-done((bf16[576,8192]{1,0:T(8,128)(2,1)}, bf16[576,8192]{1,0:T(8,128)(2,1)S(1)}, u32[]{:S(2)}) %copy-start.9) | copy-done | bytes 9437208
  143.4 3.9 %fusion.12 = f32[576,256]{1,0:T(8,128)S(1)} fusion(bf16[576,4096]{1,0:T(8,128)(2,1)} %all-gather.3.cloned.1.call-done, bf16[1,4096,256]{2,1,0:T(8,128)(2,1)S(1)} %copy-done), kind=kOutput, calls=%fused_computation.19 | convolution fusion | flops 1207959552 | bytes 7405568 | tf_op jit(solution)/shard_map/dot_general | solution.py:13
  152.3 5.5 %add_convert_fusion = bf16[768,4096]{1,0:T(8,128)(2,1)} fusion(f32[768,4096]{1,0:T(8,128)S(1)} %fusion.10, bf16[768,256]{1,0:T(8,128)(2,1)} %get-tuple-element.38, bf16[1,4096,256]{2,1,0:T(8,128)(2,1)S(1)} %copy-done.8), kind=kOutput, calls=%fused_computation | convolution fusion | flops 1616904192 | bytes 21364736 | tf_op jit(solution)/shard_map/dot_general | solution.py:13
  161.4 5.4 %collective-permute-start.21 = (bf16[260,128]{1,0:T(8,128)(2,1)}, bf16[260,128]{1,0:T(8,128)(2,1)}, u32[]{:S(2)}, u32[]{:S(2)}) collective-permute-start(bf16[260,128]{1,0:T(8,128)(2,1)} %pad_maximum_fusion.5), channel_id=1, source_target_pairs={{0,8},{8,16},{16,24},{24,0},{1,9},{9,17},{17,25},{25,1},{2,10},{10... | collective-permute-start | bytes 199688 | tf_op jit(solution)/shard_map/ppermute | solution.py:18
  170.2 55.0 %reduce-scatter.3.cloned.1.call-done = bf16[768,512]{1,0:T(8,128)(2,1)} async-done(((bf16[768,4096]{1,0:T(8,128)(2,1)}), bf16[768,512]{1,0:T(8,128)(2,1)}) %reduce-scatter.3.cloned.1.call-update) | async-done | bytes 786448 | tf_op jit(solution)/shard_map/reduce_scatter | solution.py:156
  226.6 3.4 collective-permute-start.13
  231.1 4.2 %collective-permute-done.13 = bf16[192,512]{1,0:T(8,128)(2,1)S(1)} collective-permute-done((bf16[192,512]{1,0:T(8,128)(2,1)S(1)}, bf16[192,512]{1,0:T(8,128)(2,1)S(1)}, u32[]{:S(2)}, u32[]{:S(2)}) %collective-permute-start.13) | collective-permute-done | bytes 196640 | tf_op jit(solution)/shard_map/ppermute | solution.py:18
  235.3 4.3 %collective-permute-start.23 = (bf16[260,128]{1,0:T(8,128)(2,1)}, bf16[260,128]{1,0:T(8,128)(2,1)}, u32[]{:S(2)}, u32[]{:S(2)}) collective-permute-start(bf16[260,128]{1,0:T(8,128)(2,1)} %pad_maximum_fusion.5), channel_id=1, source_target_pairs={{0,24},{8,0},{16,8},{24,16},{1,25},{9,1},{17,9},{25,17},{2,26},{10... | collective-permute-start | bytes 199688 | tf_op jit(solution)/shard_map/ppermute | solution.py:18
  239.6 7.8 %collective-permute-done.14 = bf16[192,512]{1,0:T(8,128)(2,1)S(1)} collective-permute-done((bf16[192,512]{1,0:T(8,128)(2,1)S(1)}, bf16[192,512]{1,0:T(8,128)(2,1)S(1)}, u32[]{:S(2)}, u32[]{:S(2)}) %collective-permute-start.14) | collective-permute-done | bytes 196640 | tf_op jit(solution)/shard_map/ppermute | solution.py:18
  247.5 3.3 collective-permute-start.19
  267.2 3.3 fusion.4
  270.5 3.3 fusion.5
  273.8 5.3 %all-gather.5.cloned.1.call-done = bf16[256,4096]{1,0:T(8,128)(2,1)} async-done(((bf16[256,512]{1,0:T(8,128)(2,1)}), bf16[256,4096]{1,0:T(8,128)(2,1)}) %all-gather.5.cloned.1.call-update) | async-done | bytes 2097168 | tf_op jit(solution)/shard_map/all_gather | solution.py:166
  279.1 3.7 %convolution_convert_fusion = bf16[4096,256]{1,0:T(8,128)(2,1)} fusion(bf16[256,4096]{1,0:T(8,128)(2,1)} %all-gather.5.cloned.1.call-done, f32[256,256]{0,1:T(8,128)S(1)} %fusion.27, bf16[256,256]{0,1:T(8,128)(2,1)S(1)} %copy.41), kind=kOutput, calls=%fused_computation.8 | convolution fusion | flops 538378240 | bytes 4587520 | tf_op jit(solution)/shard_map/dot_general | solution.py:13
  283.7 5.7 %fusion.6 = bf16[1,4096,256]{2,1,0:T(8,128)(2,1)} fusion(f32[4096,256]{1,0:T(8,128)S(1)} %fusion.66, bf16[576,4096]{1,0:T(8,128)(2,1)} %all-gather.3.cloned.1.call-done, bf16[768,256]{1,0:T(8,128)(2,1)S(1)} %copy-done.18), kind=kOutput, calls=%fused_computation.13 | convolution fusion | flops 1210056704 | bytes 11304960 | tf_op jit(solution)/shard_map/dot_general | solution.py:13
  290.7 3.4 collective-permute-start.16
  299.2 8.5 %collective-permute-done.18 = bf16[256,128]{1,0:T(8,128)(2,1)S(1)} collective-permute-done((bf16[256,128]{1,0:T(8,128)(2,1)S(1)}, bf16[256,128]{1,0:T(8,128)(2,1)S(1)}, u32[]{:S(2)}, u32[]{:S(2)}) %collective-permute-start.18) | collective-permute-done | bytes 65568 | tf_op jit(solution)/shard_map/ppermute | solution.py:18
  309.7 21.2 %reduce-scatter.5.cloned.1.call-done = bf16[1024,256]{1,0:T(8,128)(2,1)} async-done(((bf16[4096,256]{1,0:T(8,128)(2,1)}), bf16[1024,256]{1,0:T(8,128)(2,1)}) %reduce-scatter.5.cloned.1.call-update) | async-done | bytes 524304 | tf_op jit(solution)/shard_map/reduce_scatter | solution.py:169
  (272 shorter events, 68.3 us)
Async XLA Ops:
  7.2 104.0 %copy-start = (bf16[1,4096,256]{2,1,0:T(8,128)(2,1)S(1)}, bf16[1,4096,256]{2,1,0:T(8,128)(2,1)}, u32[]{:S(2)}) copy-start(bf16[1,4096,256]{2,1,0:T(8,128)(2,1)} %param.23) | copy-start | bytes 6291460
  7.2 136.2 %all-gather.3.cloned.1.call-start = ((), (), s32[]{:S(2)}) async-start(), calls=%async_computation.2 | async-start | bytes 5308416 | tf_op jit(solution)/shard_map/all_gather | solution.py:62
  10.5 11.0 %collective-permute-start.10 = (bf16[192,512]{1,0:T(8,128)(2,1)S(1)}, bf16[192,512]{1,0:T(8,128)(2,1)S(1)}, u32[]{:S(2)}, u32[]{:S(2)}) collective-permute-start(bf16[192,512]{1,0:T(8,128)(2,1)S(1)} %get-tuple-element.46), channel_id=1, source_target_pairs={{0,8},{8,16},{16,24},{24,0},{1,9},{9,17},{17,25},{25,1},{2,10},{10... | collective-permute-start | bytes 589832 | tf_op jit(solution)/shard_map/ppermute | solution.py:18
  13.6 15.5 %collective-permute-start.11 = (bf16[192,512]{1,0:T(8,128)(2,1)S(1)}, bf16[192,512]{1,0:T(8,128)(2,1)S(1)}, u32[]{:S(2)}, u32[]{:S(2)}) collective-permute-start(bf16[192,512]{1,0:T(8,128)(2,1)S(1)} %get-tuple-element.48), channel_id=1, source_target_pairs={{0,16},{8,24},{16,0},{24,8},{1,17},{9,25},{17,1},{25,9},{2,18},{10... | collective-permute-start | bytes 589832 | tf_op jit(solution)/shard_map/ppermute | solution.py:18
  16.2 12.9 %collective-permute-start.12 = (bf16[192,512]{1,0:T(8,128)(2,1)S(1)}, bf16[192,512]{1,0:T(8,128)(2,1)S(1)}, u32[]{:S(2)}, u32[]{:S(2)}) collective-permute-start(bf16[192,512]{1,0:T(8,128)(2,1)S(1)} %get-tuple-element.47), channel_id=1, source_target_pairs={{0,24},{8,0},{16,8},{24,16},{1,25},{9,1},{17,9},{25,17},{2,26},{10... | collective-permute-start | bytes 589832 | tf_op jit(solution)/shard_map/ppermute | solution.py:18
  30.0 195.2 %reduce-scatter.3.cloned.1.call-start = ((), (), s32[]{:S(2)}) async-start(), calls=%async_computation.3 | async-start | bytes 7077888 | tf_op jit(solution)/shard_map/reduce_scatter | solution.py:156
  30.3 72.7 %copy-start.44 = (f32[4,192]{1,0:T(4,128)}, f32[4,192]{1,0:T(4,128)S(1)}, u32[]{:S(2)}) copy-start(f32[4,192]{1,0:T(4,128)S(1)} %select_reduce_fusion) | copy-start | bytes 9220
  31.7 11.6 %collective-permute-start = (bf16[192,512]{1,0:T(8,128)(2,1)S(1)}, bf16[192,512]{1,0:T(8,128)(2,1)S(1)}, u32[]{:S(2)}, u32[]{:S(2)}) collective-permute-start(bf16[192,512]{1,0:T(8,128)(2,1)S(1)} %get-tuple-element.43), channel_id=1, source_target_pairs={{0,8},{8,16},{16,24},{24,0},{1,9},{9,17},{17,25},{25,1},{2,10},{10... | collective-permute-start | bytes 589832 | tf_op jit(solution)/shard_map/ppermute | solution.py:18
  36.4 13.6 %collective-permute-start.1 = (bf16[192,512]{1,0:T(8,128)(2,1)S(1)}, bf16[192,512]{1,0:T(8,128)(2,1)S(1)}, u32[]{:S(2)}, u32[]{:S(2)}) collective-permute-start(bf16[192,512]{1,0:T(8,128)(2,1)S(1)} %get-tuple-element.45), channel_id=1, source_target_pairs={{0,16},{8,24},{16,0},{24,8},{1,17},{9,25},{17,1},{25,9},{2,18},{10... | collective-permute-start | bytes 589832 | tf_op jit(solution)/shard_map/ppermute | solution.py:18
  38.0 12.0 %collective-permute-start.2 = (bf16[192,512]{1,0:T(8,128)(2,1)S(1)}, bf16[192,512]{1,0:T(8,128)(2,1)S(1)}, u32[]{:S(2)}, u32[]{:S(2)}) collective-permute-start(bf16[192,512]{1,0:T(8,128)(2,1)S(1)} %get-tuple-element.44), channel_id=1, source_target_pairs={{0,24},{8,0},{16,8},{24,16},{1,25},{9,1},{17,9},{25,17},{2,26},{10... | collective-permute-start | bytes 589832 | tf_op jit(solution)/shard_map/ppermute | solution.py:18
  50.1 13.3 %collective-permute-start.3 = (bf16[576,512]{1,0:T(8,128)(2,1)S(1)}, bf16[576,512]{1,0:T(8,128)(2,1)S(1)}, u32[]{:S(2)}, u32[]{:S(2)}) collective-permute-start(bf16[576,512]{1,0:T(8,128)(2,1)S(1)} %pad_maximum_fusion.3), channel_id=1, source_target_pairs={{0,1},{1,2},{2,3},{3,4},{4,5},{5,6},{6,7},{7,0},{8,9},{9,10},{10,1... | collective-permute-start | bytes 1769480 | tf_op jit(solution)/shard_map/ppermute | solution.py:65
  63.4 15.9 %collective-permute-start.4 = (bf16[576,512]{1,0:T(8,128)(2,1)S(1)}, bf16[576,512]{1,0:T(8,128)(2,1)S(1)}, u32[]{:S(2)}, u32[]{:S(2)}) collective-permute-start(bf16[576,512]{1,0:T(8,128)(2,1)S(1)} %collective-permute-done.3), channel_id=1, source_target_pairs={{0,1},{1,2},{2,3},{3,4},{4,5},{5,6},{6,7},{7,0},{8,9},{9,10},{10,1... | collective-permute-start | bytes 1769480 | tf_op jit(solution)/shard_map/ppermute | solution.py:65
  79.3 10.2 %collective-permute-start.5 = (bf16[576,512]{1,0:T(8,128)(2,1)S(1)}, bf16[576,512]{1,0:T(8,128)(2,1)S(1)}, u32[]{:S(2)}, u32[]{:S(2)}) collective-permute-start(bf16[576,512]{1,0:T(8,128)(2,1)S(1)} %collective-permute-done.4), channel_id=1, source_target_pairs={{0,1},{1,2},{2,3},{3,4},{4,5},{5,6},{6,7},{7,0},{8,9},{9,10},{10,1... | collective-permute-start | bytes 1769480 | tf_op jit(solution)/shard_map/ppermute | solution.py:65
  90.3 10.3 %collective-permute-start.6 = (bf16[576,512]{1,0:T(8,128)(2,1)S(1)}, bf16[576,512]{1,0:T(8,128)(2,1)}, u32[]{:S(2)}, u32[]{:S(2)}) collective-permute-start(bf16[576,512]{1,0:T(8,128)(2,1)S(1)} %collective-permute-done.5), channel_id=1, source_target_pairs={{0,1},{1,2},{2,3},{3,4},{4,5},{5,6},{6,7},{7,0},{8,9},{9,10},{10,1... | collective-permute-start | bytes 1769480 | tf_op jit(solution)/shard_map/ppermute | solution.py:65
  100.7 10.5 %collective-permute-start.7 = (bf16[576,512]{1,0:T(8,128)(2,1)}, bf16[576,512]{1,0:T(8,128)(2,1)}, u32[]{:S(2)}, u32[]{:S(2)}) collective-permute-start(bf16[576,512]{1,0:T(8,128)(2,1)} %collective-permute-done.6), channel_id=1, source_target_pairs={{0,1},{1,2},{2,3},{3,4},{4,5},{5,6},{6,7},{7,0},{8,9},{9,10},{10,1... | collective-permute-start | bytes 1769480 | tf_op jit(solution)/shard_map/ppermute | solution.py:65
  111.2 10.4 %collective-permute-start.8 = (bf16[576,512]{1,0:T(8,128)(2,1)}, bf16[576,512]{1,0:T(8,128)(2,1)S(1)}, u32[]{:S(2)}, u32[]{:S(2)}) collective-permute-start(bf16[576,512]{1,0:T(8,128)(2,1)} %collective-permute-done.7), channel_id=1, source_target_pairs={{0,1},{1,2},{2,3},{3,4},{4,5},{5,6},{6,7},{7,0},{8,9},{9,10},{10,1... | collective-permute-start | bytes 1769480 | tf_op jit(solution)/shard_map/ppermute | solution.py:65
  121.6 10.2 %collective-permute-start.9 = (bf16[576,512]{1,0:T(8,128)(2,1)S(1)}, bf16[576,512]{1,0:T(8,128)(2,1)S(1)}, u32[]{:S(2)}, u32[]{:S(2)}) collective-permute-start(bf16[576,512]{1,0:T(8,128)(2,1)S(1)} %collective-permute-done.8), channel_id=1, source_target_pairs={{0,1},{1,2},{2,3},{3,4},{4,5},{5,6},{6,7},{7,0},{8,9},{9,10},{10,1... | collective-permute-start | bytes 1769480 | tf_op jit(solution)/shard_map/ppermute | solution.py:65
  157.8 121.3 %all-gather.5.cloned.1.call-start = ((), (), s32[]{:S(2)}) async-start(), calls=%async_computation.4 | async-start | bytes 2359296 | tf_op jit(solution)/shard_map/all_gather | solution.py:166
  160.5 90.4 %copy-start.26 = (bf16[256,256]{0,1:T(8,128)(2,1)}, bf16[256,256]{0,1:T(8,128)(2,1)S(1)}, u32[]{:S(2)}) copy-start(bf16[256,256]{0,1:T(8,128)(2,1)S(1)} %fusion.56) | copy-start | bytes 393220
  161.4 97.3 %collective-permute-start.21 = (bf16[260,128]{1,0:T(8,128)(2,1)}, bf16[260,128]{1,0:T(8,128)(2,1)}, u32[]{:S(2)}, u32[]{:S(2)}) collective-permute-start(bf16[260,128]{1,0:T(8,128)(2,1)} %pad_maximum_fusion.5), channel_id=1, source_target_pairs={{0,8},{8,16},{16,24},{24,0},{1,9},{9,17},{17,25},{25,1},{2,10},{10... | collective-permute-start | bytes 199688 | tf_op jit(solution)/shard_map/ppermute | solution.py:18
  166.8 92.8 %collective-permute-start.22 = (bf16[260,128]{1,0:T(8,128)(2,1)}, bf16[260,128]{1,0:T(8,128)(2,1)}, u32[]{:S(2)}, u32[]{:S(2)}) collective-permute-start(bf16[260,128]{1,0:T(8,128)(2,1)} %pad_maximum_fusion.5), channel_id=1, source_target_pairs={{0,16},{8,24},{16,0},{24,8},{1,17},{9,25},{17,1},{25,9},{2,18},{10... | collective-permute-start | bytes 199688 | tf_op jit(solution)/shard_map/ppermute | solution.py:18
  170.2 86.1 %copy-start.42 = (f32[256,256]{1,0:T(8,128)}, f32[256,256]{1,0:T(8,128)S(1)}, u32[]{:S(2)}) copy-start(f32[256,256]{1,0:T(8,128)S(1)} %fusion.106) | copy-start | bytes 786436
  226.6 8.7 %collective-permute-start.13 = (bf16[192,512]{1,0:T(8,128)(2,1)S(1)}, bf16[192,512]{1,0:T(8,128)(2,1)S(1)}, u32[]{:S(2)}, u32[]{:S(2)}) collective-permute-start(bf16[192,512]{1,0:T(8,128)(2,1)S(1)} %get-tuple-element.42), channel_id=1, source_target_pairs={{0,24},{8,0},{16,8},{24,16},{1,25},{9,1},{17,9},{25,17},{2,26},{10... | collective-permute-start | bytes 589832 | tf_op jit(solution)/shard_map/ppermute | solution.py:18
  230.0 17.4 %collective-permute-start.14 = (bf16[192,512]{1,0:T(8,128)(2,1)S(1)}, bf16[192,512]{1,0:T(8,128)(2,1)S(1)}, u32[]{:S(2)}, u32[]{:S(2)}) collective-permute-start(bf16[192,512]{1,0:T(8,128)(2,1)S(1)} %get-tuple-element.41), channel_id=1, source_target_pairs={{0,16},{8,24},{16,0},{24,8},{1,17},{9,25},{17,1},{25,9},{2,18},{10... | collective-permute-start | bytes 589832 | tf_op jit(solution)/shard_map/ppermute | solution.py:18
  230.0 17.6 %collective-permute-start.15 = (bf16[192,512]{1,0:T(8,128)(2,1)S(1)}, bf16[192,512]{1,0:T(8,128)(2,1)S(1)}, u32[]{:S(2)}, u32[]{:S(2)}) collective-permute-start(bf16[192,512]{1,0:T(8,128)(2,1)S(1)} %get-tuple-element.40), channel_id=1, source_target_pairs={{0,8},{8,16},{16,24},{24,0},{1,9},{9,17},{17,25},{25,1},{2,10},{10... | collective-permute-start | bytes 589832 | tf_op jit(solution)/shard_map/ppermute | solution.py:18
  235.3 26.3 %collective-permute-start.23 = (bf16[260,128]{1,0:T(8,128)(2,1)}, bf16[260,128]{1,0:T(8,128)(2,1)}, u32[]{:S(2)}, u32[]{:S(2)}) collective-permute-start(bf16[260,128]{1,0:T(8,128)(2,1)} %pad_maximum_fusion.5), channel_id=1, source_target_pairs={{0,24},{8,0},{16,8},{24,16},{1,25},{9,1},{17,9},{25,17},{2,26},{10... | collective-permute-start | bytes 199688 | tf_op jit(solution)/shard_map/ppermute | solution.py:18
  247.4 10.8 %collective-permute-start.17 = (bf16[4,128]{1,0:T(4,128)(2,1)S(1)}, bf16[4,128]{1,0:T(4,128)(2,1)S(1)}, u32[]{:S(2)}, u32[]{:S(2)}) collective-permute-start(bf16[4,128]{1,0:T(4,128)(2,1)S(1)} %broadcast_in_dim.99), channel_id=1, source_target_pairs={{0,24},{8,0},{16,8},{24,16},{1,25},{9,1},{17,9},{25,17},{2,26},{10... | collective-permute-start | bytes 3080 | tf_op jit(solution)/shard_map/ppermute | solution.py:18
  247.5 10.7 %collective-permute-start.19 = (bf16[4,128]{1,0:T(4,128)(2,1)S(1)}, bf16[4,128]{1,0:T(4,128)(2,1)S(1)}, u32[]{:S(2)}, u32[]{:S(2)}) collective-permute-start(bf16[4,128]{1,0:T(4,128)(2,1)S(1)} %broadcast_in_dim.99), channel_id=1, source_target_pairs={{0,16},{8,24},{16,0},{24,8},{1,17},{9,25},{17,1},{25,9},{2,18},{10... | collective-permute-start | bytes 3080 | tf_op jit(solution)/shard_map/ppermute | solution.py:18
  253.2 77.7 %reduce-scatter.5.cloned.1.call-start = ((), (), s32[]{:S(2)}) async-start(), calls=%async_computation.5 | async-start | bytes 2621440 | tf_op jit(solution)/shard_map/reduce_scatter | solution.py:169
  290.7 8.5 %collective-permute-start.16 = (bf16[256,128]{1,0:T(8,128)(2,1)S(1)}, bf16[256,128]{1,0:T(8,128)(2,1)S(1)}, u32[]{:S(2)}, u32[]{:S(2)}) collective-permute-start(bf16[256,128]{1,0:T(8,128)(2,1)S(1)} %convolution_convert_fusion.4), channel_id=1, source_target_pairs={{0,24},{8,0},{16,8},{24,16},{1,25},{9,1},{17,9},{25,17},{2,26},{10... | collective-permute-start | bytes 196616 | tf_op jit(solution)/shard_map/ppermute | solution.py:18
  294.1 13.6 %collective-permute-start.18 = (bf16[256,128]{1,0:T(8,128)(2,1)S(1)}, bf16[256,128]{1,0:T(8,128)(2,1)S(1)}, u32[]{:S(2)}, u32[]{:S(2)}) collective-permute-start(bf16[256,128]{1,0:T(8,128)(2,1)S(1)} %convolution_convert_fusion.4), channel_id=1, source_target_pairs={{0,16},{8,24},{16,0},{24,8},{1,17},{9,25},{17,1},{25,9},{2,18},{10... | collective-permute-start | bytes 196616 | tf_op jit(solution)/shard_map/ppermute | solution.py:18
  294.1 13.6 %collective-permute-start.20 = (bf16[256,128]{1,0:T(8,128)(2,1)S(1)}, bf16[256,128]{1,0:T(8,128)(2,1)S(1)}, u32[]{:S(2)}, u32[]{:S(2)}) collective-permute-start(bf16[256,128]{1,0:T(8,128)(2,1)S(1)} %convolution_convert_fusion.4), channel_id=1, source_target_pairs={{0,8},{8,16},{16,24},{24,0},{1,9},{9,17},{17,25},{25,1},{2,10},{10... | collective-permute-start | bytes 196616 | tf_op jit(solution)/shard_map/ppermute | solution.py:18
  (58 other events, 514.9 us)
Sparse Core Ops, SparseCore 0:
  30.1 48.3 all-gather.2
  157.9 67.2 reduce-scatter.2
  253.3 25.7 all-gather.4
  283.0 47.8 reduce-scatter.4
